TPU v7x, 32 devices: a whole 2x2x4 slice. The times are simulated.
32 devices in a mesh: st: 8 (over z, y), tp: 4 (over x, core).
Axes of the slice: x: 2, y: 2, z: 4, core: 2. Of those that a mesh axis runs over, the one named last changes fastest.
Arguments:
- tokens: bfloat16 [3072, 2048], P('st', 'tp'), may hold values from -6 to 6
- cotangent: bfloat16 [3072, 1024], P('st', 'tp'), may hold values from -48 to 48
- mix_query: bfloat16 [3072, 1024], P('st', 'tp'), may hold values from -6 to 6
- mix_key: bfloat16 [3072, 1024], P('st', 'tp'), may hold values from -6 to 6
- mix_value: bfloat16 [3072, 1024], P('st', 'tp'), may hold values from -24 to 24
- beta_pre: float32 [8, 3072], P('tp', 'st'), may hold values from -9 to 9
- decay_pre: float32 [8, 3072], P('tp', 'st'), may hold values from -8 to 6
- decay_rate: float32 [8], P('tp'), may hold values from 0.001 to 0.06
- passages: bfloat16 [128, 64, 2048], P('st'), may hold values from -6 to 6
- passage_ids: int32 [48, 4], P('st'), may hold values from 0 to 127, as said below
- query_weight: bfloat16 [2048, 1024], P(None, 'tp'), may hold values from -0.125 to 0.125
- key_weight: bfloat16 [2048, 1024], P(None, 'tp'), may hold values from -0.125 to 0.125
- value_weight: bfloat16 [2048, 1024], P(None, 'tp'), may hold values from -0.125 to 0.125
- gate_weight: bfloat16 [4, 2048], P('tp'), may hold values from -0.125 to 0.125
Outputs:
- token_grad: bfloat16 [3072, 2048], P('st', 'tp')
- passage_grad: bfloat16 [128, 64, 2048], P('st', None, 'tp')
- key_weight_grad: float32 [2048, 1024], P('st', 'tp')
Inputs may be any that keep to these rules, and one draw needn't show every extreme that they name: Passage p is stored on index p // 16 of st. The rows of passage_ids read by one index of st name at most 3 passages stored on any one index of st, and exactly 3 on some.
All inputs are finite; a program needn't handle non-finite values.
Results may differ from a plain program's by a relative error of at most 0.012.
The roundings to bfloat16 on the way count: a program that leaves them out, or rounds other values in their place, can miss the bound.
Values may be sent and summed in bfloat16 or wider, within the bound.
A program may use at most 128 MiB of HBM per device.

v0:
```python
import functools

import jax
import jax.numpy as jnp
from jax import lax
from jax.experimental import pallas as pl
from jax.experimental.pallas import tpu as pltpu
from jax.sharding import PartitionSpec as P

SPAN = 64


NORM_FLOOR = 1.0
SCORE_GAIN = 4.0
HIGHEST = lax.Precision.HIGHEST
CONTRACT_LAST = (((1,), (1,)), ((), ()))
CONTRACT_FIRST = (((0,), (0,)), ((), ()))

MESH = pl.DeviceIdType.MESH
VMEM_SPEC = pl.BlockSpec(memory_space=pltpu.VMEM)
DMA = pltpu.SemaphoreType.DMA
CHUNK = 256


def tp_places():
    place = lax.axis_index("tp")
    parity = lax.rem(place, 2)
    half = place // 2
    return place, parity, half, place + 1 - 2 * parity, lax.rem(place + 2, 4)


def st_peer(me, step, st_count):
    half = st_count // 2
    side, place = me // half, lax.rem(me, half)
    if step <= half:
        return (1 - side) * half + lax.rem(place + step - 1, half)
    return side * half + lax.rem(place + step - half, half)


def meet(st_count, with_st, with_tp=True):
    barrier = pltpu.get_barrier_semaphore()
    _, _, _, partner, far = tp_places()
    for other in (partner, far) if with_tp else ():
        pl.semaphore_signal(barrier, inc=1, device_id={"tp": other}, device_id_type=MESH)
    total = 2 if with_tp else 0
    if with_st:
        me = lax.axis_index("st")
        for step in range(1, st_count):
            pl.semaphore_signal(
                barrier,
                inc=1,
                device_id={"st": st_peer(me, step, st_count)},
                device_id_type=MESH,
            )
        total += st_count - 1
    pl.semaphore_wait(barrier, total)


def scatter_sum(term, out_ref, chunks, first_send, first_recv, kept, second_send, second_recv, sems):
    _, parity, half, partner, far = tp_places()
    send_a, recv_a, send_b, recv_b = sems
    rows = out_ref.shape[0] // chunks

    def pair_copy(k, i):
        return pltpu.make_async_remote_copy(
            src_ref=first_send.at[k, i],
            dst_ref=first_recv.at[k, i],
            send_sem=send_a.at[k, i],
            recv_sem=recv_a.at[k, i],
            device_id={"tp": partner},
            device_id_type=MESH,
        )

    def far_copy(k):
        return pltpu.make_async_remote_copy(
            src_ref=second_send.at[k],
            dst_ref=second_recv.at[k],
            send_sem=send_b.at[k],
            recv_sem=recv_b.at[k],
            device_id={"tp": far},
            device_id_type=MESH,
        )

    def pass_on(k):
        pair_copy(k, 0).wait_recv()
        second_send[k] = (
            kept[k, 0].astype(jnp.float32) + first_recv[k, 0].astype(jnp.float32)
        ).astype(jnp.bfloat16)
        far_copy(k).start()

    for k in range(chunks):
        for i in range(2):
            column = 2 * (1 - half if i == 0 else half)
            first_send[k, i] = term(k, column + 1 - parity).astype(jnp.bfloat16)
            pair_copy(k, i).start()
            kept[k, i] = term(k, column + parity).astype(jnp.bfloat16)
            if i == 0 and k >= 1:
                pass_on(k - 1)
    pass_on(chunks - 1)
    for k in range(chunks):
        pair_copy(k, 1).wait_recv()
        far_copy(k).wait_recv()
        out_ref[pl.ds(k * rows, rows), :] = (
            kept[k, 1].astype(jnp.float32)
            + first_recv[k, 1].astype(jnp.float32)
            + second_recv[k].astype(jnp.float32)
        ).astype(out_ref.dtype)
    for k in range(chunks):
        pair_copy(k, 0).wait_send()
        pair_copy(k, 1).wait_send()
        far_copy(k).wait_send()


def scatter_scratch(chunks, rows, width):
    return [
        pltpu.VMEM((chunks, 2, rows, width), jnp.bfloat16),
        pltpu.VMEM((chunks, 2, rows, width), jnp.bfloat16),
        pltpu.VMEM((chunks, 2, rows, width), jnp.bfloat16),
        pltpu.VMEM((chunks, rows, width), jnp.bfloat16),
        pltpu.VMEM((chunks, rows, width), jnp.bfloat16),
        DMA((chunks, 2)),
        DMA((chunks, 2)),
        DMA((chunks,)),
        DMA((chunks,)),
    ]


def project_kernel(
    st_count,
    ids_ref,
    rows_hbm,
    kw_ref,
    vw_ref,
    ids_all_ref,
    key_ref,
    packed_ref,
    rows_ref,
    rows_sem,
    id_send,
    id_recv,
):
    me = lax.axis_index("st")
    head_dim = kw_ref.shape[1]
    chunks = rows_ref.shape[0] // CHUNK

    def rows_copy(k):
        here = pl.ds(k * CHUNK, CHUNK)
        return pltpu.make_async_copy(rows_hbm.at[here, :], rows_ref.at[here, :], rows_sem.at[k])

    for k in range(chunks):
        rows_copy(k).start()
    meet(st_count, True, False)

    def id_copy(step):
        return pltpu.make_async_remote_copy(
            src_ref=ids_ref,
            dst_ref=ids_all_ref.at[me],
            send_sem=id_send.at[step],
            recv_sem=id_recv.at[step],
            device_id={"st": st_peer(me, step, st_count)},
            device_id_type=MESH,
        )

    for step in range(1, st_count):
        id_copy(step).start()
    ids_all_ref[pl.ds(me, 1)] = ids_ref[...][None]

    for k in range(chunks):
        rows_copy(k).wait()
        here = pl.ds(k * CHUNK, CHUNK)
        block = rows_ref[here, :]
        key_low = jnp.dot(block, kw_ref[...], preferred_element_type=jnp.float32).astype(
            jnp.bfloat16
        )
        key_ref[here, :] = key_low
        key_float = key_low.astype(jnp.float32)
        scale = lax.rsqrt(jnp.mean(key_float * key_float, axis=-1, keepdims=True) + NORM_FLOOR)
        packed_ref[here, pl.ds(0, head_dim)] = (key_float * scale).astype(jnp.bfloat16)
        packed_ref[here, pl.ds(head_dim, head_dim)] = jnp.dot(
            block, vw_ref[...], preferred_element_type=jnp.float32
        ).astype(jnp.bfloat16)

    for step in range(1, st_count):
        id_copy(step).wait()


def project_call(st_count, ids_padded, flat_rows, key_weight, value_weight):
    head_dim = key_weight.shape[1]
    total_rows = flat_rows.shape[0]
    return pl.pallas_call(
        functools.partial(project_kernel, st_count),
        out_shape=(
            jax.ShapeDtypeStruct((st_count, *ids_padded.shape), jnp.int32),
            jax.ShapeDtypeStruct((total_rows, head_dim), jnp.bfloat16),
            jax.ShapeDtypeStruct((total_rows, 2 * head_dim), jnp.bfloat16),
        ),
        in_specs=[VMEM_SPEC, pl.BlockSpec(memory_space=pl.ANY), VMEM_SPEC, VMEM_SPEC],
        out_specs=(VMEM_SPEC,) * 3,
        scratch_shapes=[
            pltpu.VMEM(flat_rows.shape, jnp.bfloat16),
            DMA((total_rows // CHUNK,)),
            DMA((st_count,)),
            DMA((st_count,)),
        ],
        compiler_params=pltpu.CompilerParams(collective_id=0, has_side_effects=True),
        name="ids_project",
    )(ids_padded, flat_rows, key_weight, value_weight)


def settle_kernel(*refs):
    count = len(refs) // 2
    for source, target in zip(refs[:count], refs[count:]):
        target[...] = source[...]


def settle_call(*arrays):
    return pl.pallas_call(
        settle_kernel,
        out_shape=tuple(jax.ShapeDtypeStruct(x.shape, x.dtype) for x in arrays),
        in_specs=[VMEM_SPEC] * len(arrays),
        out_specs=(VMEM_SPEC,) * len(arrays),
        name="settle",
    )(*arrays)


def exact_dot(left, right, dims=(((1,), (0,)), ((), ()))):
    return lax.dot_general(
        left, right, dims, precision=HIGHEST, preferred_element_type=jnp.float32
    )


def mixer_span(queries, keys_in, values_in, strength, log_decay, state):
    span = queries.shape[0]
    row_at = lax.broadcasted_iota(jnp.int32, (span, span), 0)
    col_at = lax.broadcasted_iota(jnp.int32, (span, span), 1)
    inclusive = row_at >= col_at
    unit_eye = jnp.where(row_at == col_at, 1.0, 0.0)
    decay_row = jnp.sum(unit_eye * log_decay, axis=0, keepdims=True)
    cum_row = jnp.sum(jnp.where(row_at <= col_at, log_decay, 0.0), axis=0, keepdims=True)
    cum_col = jnp.sum(jnp.where(inclusive, decay_row, 0.0), axis=1, keepdims=True)
    total = jnp.sum(log_decay, axis=0, keepdims=True)
    decay_map = jnp.exp(jnp.where(inclusive, cum_col - cum_row, -1e30))
    queries = (
        queries
        * lax.rsqrt(jnp.sum(queries * queries, axis=-1, keepdims=True) + NORM_FLOOR)
        * queries.shape[-1] ** (-0.5)
    )
    keys_in = keys_in * lax.rsqrt(jnp.sum(keys_in * keys_in, axis=-1, keepdims=True) + NORM_FLOOR)
    power = jnp.where(
        row_at > col_at, strength * exact_dot(keys_in, keys_in, CONTRACT_LAST) * decay_map, 0.0
    )
    inverse = unit_eye - power
    for _ in range(span.bit_length() - 2):
        power = exact_dot(power, power)
        inverse = exact_dot(inverse, unit_eye + power)
    attend = exact_dot(queries, keys_in, CONTRACT_LAST) * decay_map
    fresh = exact_dot(inverse, values_in * strength)
    correction = exact_dot(inverse, keys_in * (strength * jnp.exp(cum_col)))
    new_values = fresh - exact_dot(correction, state)
    output = exact_dot(queries * jnp.exp(cum_col), state) + exact_dot(attend, new_values)
    state = state * jnp.exp(total) + exact_dot(
        keys_in * jnp.exp(total - cum_col), new_values, CONTRACT_FIRST
    )
    return output, state


def main_kernel(
    st_count,
    sizes,
    local_ref,
    slot_ref,
    request_ref,
    rate_ref,
    code_ref,
    own_ref,
    packed_ref,
    key_ref,
    cot_ref,
    mq_ref,
    mk_ref,
    mv_ref,
    beta_ref,
    decay_ref,
    qw_ref,
    gate_ref,
    kw_ref,
    vw_ref,
    rows_hbm,
    tok_out,
    out_ref,
    weight_ref,
    tok_ref,
    tok_send,
    tok_recv,
    gw_ref,
    turned,
    rows_ref,
    rows_sem,
    send_buf,
    arrived,
    reply_rows,
    reply_send,
    reply_recv,
    x_sems,
    query_low,
    query_hat,
    query_grad,
    gate_grad,
    gate_open,
    mixed,
    states,
    block_kv,
    key_grad,
    value_grad,
    weight_send,
    weight_recv,
    w_send,
    w_recv,
    *scratch,
):
    cap, per_block, tok_chunks, row_chunks = sizes
    me = lax.axis_index("st")
    slot_total, span_rows, _ = send_buf.shape
    head_dim = key_ref.shape[1]
    part = weight_ref.shape[0]
    blocks_n = slot_ref.shape[0] // per_block
    block_rows = tok_ref.shape[0] // blocks_n
    heads_n = beta_ref.shape[0]
    mix_dim = mq_ref.shape[1] // heads_n
    score_scale = SCORE_GAIN * head_dim ** (-0.5)
    rows_copy = pltpu.make_async_copy(rows_hbm, rows_ref, rows_sem)
    rows_copy.start()
    meet(st_count, True)

    def exchange(lane, source, target, step):
        peer = st_peer(me, step, st_count)
        return pltpu.make_async_remote_copy(
            src_ref=source.at[pl.ds(peer * cap, cap)],
            dst_ref=target.at[pl.ds(me * cap, cap)],
            send_sem=x_sems.at[lane, 0, step],
            recv_sem=x_sems.at[lane, 1, step],
            device_id={"st": peer},
            device_id_type=MESH,
        )

    place, _, _, partner, far = tp_places()
    own_width = own_ref.shape[1]

    def tok_columns(which):
        return pl.ds(pl.multiple_of(which * own_width, own_width), own_width)

    def tok_copy(lane, source, which, target):
        return pltpu.make_async_remote_copy(
            src_ref=source,
            dst_ref=tok_ref.at[:, tok_columns(which)],
            send_sem=tok_send.at[lane],
            recv_sem=tok_recv.at[lane],
            device_id={"tp": target},
            device_id_type=MESH,
        )

    to_partner = tok_copy(0, own_ref, place, partner)
    to_far = tok_copy(1, own_ref, place, far)
    onward = tok_copy(2, tok_ref.at[:, tok_columns(far)], far, partner)
    to_far.start()
    for step in range(1, st_count):
        peer = st_peer(me, step, st_count)
        for c in range(cap):
            send_buf[peer * cap + c] = packed_ref[local_ref[peer * cap + c]]
        exchange(0, send_buf, arrived, step).start()
    for c in range(cap):
        arrived[me * cap + c] = packed_ref[local_ref[me * cap + c]]

    to_partner.start()
    tok_ref[:, tok_columns(place)] = own_ref[...]
    gw_ref[...] = gate_ref[...].astype(jnp.float32)
    turned[...] = jnp.transpose(
        jnp.concatenate(
            [
                beta_ref[...],
                decay_ref[...],
                jnp.zeros((8 - 2 * heads_n, beta_ref.shape[1]), jnp.float32),
            ],
            axis=0,
        )
    )
    states[...] = jnp.zeros_like(states)

    def mix(b):
        here = pl.ds(pl.multiple_of(b * SPAN, SPAN), SPAN)
        for m in range(heads_n):
            cols = pl.ds(m * mix_dim, mix_dim)
            raw = turned[here, heads_n + m : heads_n + m + 1]
            softplus = jnp.maximum(raw, 0.0) + jnp.log1p(jnp.exp(-jnp.abs(raw)))
            mixed[here, cols], states[m] = mixer_span(
                mq_ref[here, cols].astype(jnp.float32),
                mk_ref[here, cols].astype(jnp.float32),
                mv_ref[here, cols].astype(jnp.float32),
                jax.nn.sigmoid(turned[here, m : m + 1]),
                -rate_ref[m] * softplus,
                states[m],
            )

    spans_n = tok_ref.shape[0] // SPAN
    pl.loop(0, spans_n // 2)(mix)
    to_far.wait_recv()
    onward.start()
    pl.loop(spans_n // 2, spans_n)(mix)
    to_partner.wait_recv()
    onward.wait_recv()

    @pl.loop(0, blocks_n)
    def _(b):
        here = pl.ds(pl.multiple_of(b * block_rows, block_rows), block_rows)
        low = jnp.dot(tok_ref[here, :], qw_ref[...], preferred_element_type=jnp.float32).astype(
            jnp.bfloat16
        )
        query_low[here, :] = low
        low = low.astype(jnp.float32)
        scale = lax.rsqrt(jnp.mean(low * low, axis=-1, keepdims=True) + NORM_FLOOR)
        query_hat[here, :] = (low * scale).astype(jnp.bfloat16)
        gate_open[here, :] = jax.nn.sigmoid(
            jnp.sum(tok_ref[here, :].astype(jnp.float32) * gw_ref[...], axis=-1, keepdims=True)
        )

    for step in range(1, st_count):
        exchange(0, send_buf, arrived, step).wait_recv()

    @pl.loop(0, blocks_n)
    def _(b):
        here = pl.ds(pl.multiple_of(b * block_rows, block_rows), block_rows)
        for j in range(per_block):
            block_kv[pl.ds(j * span_rows, span_rows), :] = arrived[slot_ref[b * per_block + j]]
        keys = block_kv[:, :head_dim]
        values = block_kv[:, head_dim:]
        q_hat = query_hat[here, :]
        opened = gate_open[here, :]
        cot = cot_ref[here, :].astype(jnp.float32)
        grad_ret = (opened * cot).astype(jnp.bfloat16)
        exp_scores = jnp.exp(
            lax.dot_general(q_hat, keys, CONTRACT_LAST, preferred_element_type=jnp.float32)
            * score_scale
        )
        probs = exp_scores / jnp.sum(exp_scores, axis=-1, keepdims=True)
        probs_low = probs.astype(jnp.bfloat16)
        retrieved = jnp.dot(probs_low, values, preferred_element_type=jnp.float32)
        gate_grad[here, :] = (
            jnp.sum(cot * (retrieved - mixed[here, :]), axis=-1, keepdims=True)
            * opened
            * (1.0 - opened)
        )
        grad_probs = lax.dot_general(
            grad_ret, values, CONTRACT_LAST, preferred_element_type=jnp.float32
        )
        score_grad = (
            probs * (grad_probs - jnp.sum(grad_probs * probs, axis=-1, keepdims=True))
        ).astype(jnp.bfloat16)
        key_term = (
            score_scale
            * lax.dot_general(score_grad, q_hat, CONTRACT_FIRST, preferred_element_type=jnp.float32)
        ).astype(jnp.bfloat16)
        value_term = lax.dot_general(
            probs_low, grad_ret, CONTRACT_FIRST, preferred_element_type=jnp.float32
        ).astype(jnp.bfloat16)
        for j in range(per_block):
            piece = slice(j * span_rows, (j + 1) * span_rows)
            reply_rows[b * per_block + j, :, pl.ds(0, head_dim)] = key_term[piece]
            reply_rows[b * per_block + j, :, pl.ds(head_dim, head_dim)] = value_term[piece]
        hat_grad = score_scale * jnp.dot(score_grad, keys, preferred_element_type=jnp.float32)
        low = query_low[here, :].astype(jnp.float32)
        scale = lax.rsqrt(jnp.mean(low * low, axis=-1, keepdims=True) + NORM_FLOOR)
        query_grad[here, :] = (
            scale * hat_grad
            - scale * scale * scale * low * jnp.mean(low * hat_grad, axis=-1, keepdims=True)
        ).astype(jnp.bfloat16)

    for step in range(1, st_count):
        peer = st_peer(me, step, st_count)
        for c in range(cap):
            reply_send[peer * cap + c] = reply_rows[request_ref[peer * cap + c]]
        exchange(1, reply_send, reply_recv, step).start()
    for c in range(cap):
        reply_recv[me * cap + c] = reply_rows[request_ref[me * cap + c]]

    tok_width = tok_out.shape[1]
    tok_rows = tok_out.shape[0] // tok_chunks

    def token_term(k, which):
        here = pl.ds(k * tok_rows, tok_rows)
        cols = pl.ds(pl.multiple_of(which * tok_width, tok_width), tok_width)
        return (
            lax.dot_general(
                query_grad[here, :],
                qw_ref[cols, :],
                CONTRACT_LAST,
                preferred_element_type=jnp.float32,
            )
            + gate_grad[here, :] * gw_ref[:, cols]
        )

    scatter_sum(token_term, tok_out, tok_chunks, *scratch[:5], scratch[5:9])

    for step in range(1, st_count):
        exchange(1, reply_send, reply_recv, step).wait_recv()

    @pl.loop(0, out_ref.shape[0] // CHUNK)
    def _(k):
        here = pl.ds(pl.multiple_of(k * CHUNK, CHUNK), CHUNK)
        row_at = lax.broadcasted_iota(jnp.int32, (CHUNK, code_ref.shape[1]), 0) + k * CHUNK
        pick = jnp.where(row_at == code_ref[...], 1.0, 0.0).astype(jnp.bfloat16)
        summed = jnp.dot(
            pick,
            reply_recv[...].reshape(slot_total * span_rows, 2 * head_dim),
            preferred_element_type=jnp.float32,
        )
        hat_grad = summed[:, :head_dim]
        key_float = key_ref[here, :].astype(jnp.float32)
        scale = lax.rsqrt(jnp.mean(key_float * key_float, axis=-1, keepdims=True) + NORM_FLOOR)
        key_grad[here, :] = (
            scale * hat_grad
            - scale * scale * scale
            * key_float
            * jnp.mean(key_float * hat_grad, axis=-1, keepdims=True)
        ).astype(jnp.bfloat16)
        value_grad[here, :] = summed[:, head_dim:].astype(jnp.bfloat16)

    rows_copy.wait()

    def own_part(which):
        return weight_send.at[pl.ds(pl.multiple_of(which * part, part), part), :]

    def weight_copy(step):
        target = st_peer(me, step, st_count)
        return pltpu.make_async_remote_copy(
            src_ref=own_part(target),
            dst_ref=weight_recv.at[step],
            send_sem=w_send.at[step],
            recv_sem=w_recv.at[step],
            device_id={"st": target},
            device_id_type=MESH,
        )

    @pl.loop(0, weight_send.shape[0] // CHUNK)
    def _(k):
        here = pl.ds(pl.multiple_of(k * CHUNK, CHUNK), CHUNK)
        weight_send[here, :] = lax.dot_general(
            rows_ref[:, here], key_grad[...], CONTRACT_FIRST, preferred_element_type=jnp.float32
        ).astype(jnp.bfloat16)

    for step in range(1, st_count):
        weight_copy(step).start()

    width = out_ref.shape[1]
    rows = out_ref.shape[0] // row_chunks

    def row_term(k, which):
        here = pl.ds(k * rows, rows)
        cols = pl.ds(pl.multiple_of(which * width, width), width)
        return lax.dot_general(
            key_grad[here, :], kw_ref[cols, :], CONTRACT_LAST, preferred_element_type=jnp.float32
        ) + lax.dot_general(
            value_grad[here, :], vw_ref[cols, :], CONTRACT_LAST, preferred_element_type=jnp.float32
        )

    scatter_sum(row_term, out_ref, row_chunks, *scratch[9:14], scratch[14:18])
    weight_ref[...] = own_part(me)[...].astype(jnp.float32)
    for step in range(1, st_count):
        weight_copy(step).wait_recv()
        weight_ref[...] += weight_recv[step].astype(jnp.float32)
    for step in range(1, st_count):
        weight_copy(step).wait_send()
        exchange(0, send_buf, arrived, step).wait_send()
        exchange(1, reply_send, reply_recv, step).wait_send()
    to_partner.wait_send()
    to_far.wait_send()
    onward.wait_send()


def main_call(st_count, cap, per_block, span_rows, *operands):
    slot_local, tok, key_low, cot = operands[0], operands[5], operands[7], operands[8]
    flat_rows = operands[-1]
    heads_n = operands[12].shape[0]
    slot_total = slot_local.shape[0]
    tok_rows, model_width = tok.shape[0], flat_rows.shape[1]
    rows, head_dim = key_low.shape
    width = model_width // 4
    part = model_width // st_count
    tok_chunks, row_chunks = 3, 4
    mix_dim = cot.shape[1] // heads_n
    slots = pltpu.VMEM((slot_total, span_rows, 2 * head_dim), jnp.bfloat16)
    smem = pl.BlockSpec(memory_space=pltpu.SMEM)
    return pl.pallas_call(
        functools.partial(main_kernel, st_count, (cap, per_block, tok_chunks, row_chunks)),
        out_shape=(
            jax.ShapeDtypeStruct((tok_rows, width), jnp.bfloat16),
            jax.ShapeDtypeStruct((rows, width), jnp.bfloat16),
            jax.ShapeDtypeStruct((part, head_dim), jnp.float32),
        ),
        in_specs=[smem] * 4 + [VMEM_SPEC] * 14 + [pl.BlockSpec(memory_space=pl.ANY)],
        out_specs=(VMEM_SPEC,) * 3,
        scratch_shapes=[
            pltpu.VMEM((tok_rows, model_width), jnp.bfloat16),
            DMA((3,)),
            DMA((3,)),
            pltpu.VMEM((1, model_width), jnp.float32),
            pltpu.VMEM((tok_rows, 8), jnp.float32),
            pltpu.VMEM(flat_rows.shape, jnp.bfloat16),
            DMA(()),
            slots,
            slots,
            pltpu.VMEM((operands[1].shape[0], span_rows, 2 * head_dim), jnp.bfloat16),
            slots,
            slots,
            DMA((2, 2, st_count)),
            pltpu.VMEM((tok_rows, head_dim), jnp.bfloat16),
            pltpu.VMEM((tok_rows, head_dim), jnp.bfloat16),
            pltpu.VMEM((tok_rows, head_dim), jnp.bfloat16),
            pltpu.VMEM((tok_rows, 1), jnp.float32),
            pltpu.VMEM((tok_rows, 1), jnp.float32),
            pltpu.VMEM((tok_rows, head_dim), jnp.float32),
            pltpu.VMEM((heads_n, mix_dim, mix_dim), jnp.float32),
            pltpu.VMEM((per_block * span_rows, 2 * head_dim), jnp.bfloat16),
            pltpu.VMEM((rows, head_dim), jnp.bfloat16),
            pltpu.VMEM((rows, head_dim), jnp.bfloat16),
            pltpu.VMEM((model_width, head_dim), jnp.bfloat16),
            pltpu.VMEM((st_count, part, head_dim), jnp.bfloat16),
            DMA((st_count,)),
            DMA((st_count,)),
            *scatter_scratch(tok_chunks, tok_rows // tok_chunks, width),
            *scatter_scratch(row_chunks, rows // row_chunks, width),
        ],
        compiler_params=pltpu.CompilerParams(collective_id=1, has_side_effects=True),
        name="exchange_attend",
    )(*operands)


def request_slots(id_rows, pass_count):
    owners = id_rows // pass_count
    local_idx = id_rows % pass_count
    req_count = id_rows.shape[-1]
    req_order = jnp.arange(req_count, dtype=jnp.int32)
    earlier = (owners[..., :, None] == owners[..., None, :]) & (
        req_order[None, :] < req_order[:, None]
    )
    ranks = jnp.sum(earlier.astype(jnp.int32), axis=-1, dtype=jnp.int32)
    return (owners, local_idx, ranks)


def body(
    tokens,
    cotangent,
    mix_query,
    mix_key,
    mix_value,
    beta_pre,
    decay_pre,
    decay_rate,
    passages,
    passage_ids,
    query_weight,
    key_weight,
    value_weight,
    gate_weight,
):
    model_width = query_weight.shape[0]
    head_dim = query_weight.shape[1]
    pass_local = passages.shape[0]
    span_rows = passages.shape[1]
    blocks_n = passage_ids.shape[0]
    per_block = passage_ids.shape[1]
    req_count = blocks_n * per_block
    st_count = lax.axis_size("st")
    my_owner = lax.axis_index("st")
    cap_count = max(1, req_count // st_count)
    slot_total = st_count * cap_count
    req_order = jnp.arange(req_count, dtype=jnp.int32)
    flat_rows = passages.reshape(pass_local * span_rows, model_width)
    flat_ids = passage_ids.reshape(1, req_count)
    ids_padded = jnp.pad(flat_ids, ((0, 7), (0, -req_count % 128)))
    ids_all, key_low, packed = project_call(
        st_count, ids_padded, flat_rows, key_weight, value_weight
    )
    every_id = ids_all[:, 0, :req_count]
    packed = packed.reshape(pass_local, span_rows, 2 * head_dim)
    all_owner, all_local, all_rank = request_slots(every_id, pass_local)
    cap_iota = jnp.arange(cap_count, dtype=jnp.int32)
    wanted = (all_owner == my_owner)[:, None, :] & (all_rank[:, None, :] == cap_iota[None, :, None])
    slot_used = jnp.any(wanted, axis=-1)
    slot_local = jnp.sum(jnp.where(wanted, all_local[:, None, :], 0), axis=-1, dtype=jnp.int32)
    own_owner, _, own_rank = request_slots(passage_ids.reshape(req_count), pass_local)
    slot_of = own_owner * cap_count + own_rank
    slot_match = slot_of[None, :] == jnp.arange(slot_total, dtype=jnp.int32)[:, None]
    slot_req = jnp.sum(jnp.where(slot_match, req_order[None, :], 0), axis=-1, dtype=jnp.int32)
    slot_row = jnp.where(slot_used, slot_local * span_rows, -span_rows).reshape(slot_total, 1)
    code = (slot_row + jnp.arange(span_rows, dtype=jnp.int32)[None, :]).reshape(1, -1)
    token_grad, passage_grad, key_weight_grad = main_call(
        st_count,
        cap_count,
        per_block,
        span_rows,
        slot_local.reshape(slot_total),
        slot_of,
        slot_req,
        decay_rate,
        code,
        tokens,
        packed,
        key_low,
        cotangent,
        mix_query,
        mix_key,
        mix_value,
        beta_pre,
        decay_pre,
        query_weight,
        gate_weight,
        key_weight,
        value_weight,
        flat_rows,
    )
    token_grad, passage_grad, key_weight_grad = settle_call(
        token_grad, passage_grad, key_weight_grad
    )
    passage_grad = passage_grad.reshape(pass_local, span_rows, -1)
    return (token_grad, passage_grad, key_weight_grad)


def solution(mesh):
    placed = (
        P("st", "tp"),
        P("st", "tp"),
        P("st", "tp"),
        P("st", "tp"),
        P("st", "tp"),
        P("tp", "st"),
        P("tp", "st"),
        P("tp"),
        P("st", None, None),
        P("st", None),
        P(None, "tp"),
        P(None, "tp"),
        P(None, "tp"),
        P("tp", None),
    )
    return jax.shard_map(
        body,
        mesh=mesh,
        in_specs=placed,
        out_specs=(P("st", "tp"), P("st", None, "tp"), P("st", "tp")),
        check_vma=False,
    )
```

profile of v0, /device:TPU:20, one launch (start us, length us, event | category | flops | bytes accessed | tf_op | source)
XLA Modules:
  0.0 145.8 jit_solution(9542461110369562194)
XLA Ops:
  0.6 0.8 copy.21
  1.4 0.1 reshape.171
  1.5 0.1 reshape.168
  1.6 0.2 convert_reduce_fusion.1
  1.8 0.0 copy-start.1
  1.8 0.6 select_reduce_fusion.request_ref
  2.4 0.6 pad.4.ids_ref
  3.0 9.4 %ids_project.1 = (s32[8,8,128]{2,1,0:T(8,128)}, bf16[1024,256]{1,0:T(8,128)(2,1)}, bf16[1024,512]{1,0:T(8,128)(2,1)}) custom-call(s32[8,128]{1,0:T(8,128)} %pad.4.ids_ref, bf16[1024,2048]{1,0:T(8,128)(2,1)} %bitcast.9, bf16[2048,256]{1,0:T(8,128)(2,1)} %kw_ref.3, bf16[2048,256]{1,0:T(8,128)(2,1)} %vw_ref.3), custom_call_target="tpu_custom_call" | custom-call | tf_op jit(solution)/shard_map/ids_project/pallas_call | solution.py:190
  12.4 0.8 slice.3
  13.2 0.8 broadcast_compare_fusion
  14.0 0.3 convert_reduce_fusion
  14.3 0.2 fusion.1
  14.4 0.1 copy.24
  14.5 0.1 reduce_or.12
  14.7 0.1 select_reduce_fusion.1
  14.8 0.1 copy.22
  14.9 0.1 reshape.170.local_ref
  15.0 0.0 copy-start
  15.0 0.1 iota_add_fusion
  15.1 0.7 add.59.code_ref
  15.7 0.0 copy-done.1
  15.7 0.0 copy-done
  15.7 127.4 %exchange_attend.1 = (bf16[384,512]{1,0:T(8,128)(2,1)}, bf16[1024,512]{1,0:T(8,128)(2,1)}, f32[256,256]{1,0:T(8,128)}) custom-call(s32[24]{0:T(128)} %copy-done, s32[24]{0:T(128)} %copy-done.1, s32[24]{0:T(128)} %select_reduce_fusion.request_ref, f32[2]{0:T(128)} %rate_ref.1, s32[1,1536]{1,0:T(1,128)} %add.59.code_ref, bf16[384,512]{1,0:T(8,128)(2,1)} %own_ref.1, ...), custom_call_target="tpu_custom_call" | custom-call | tf_op jit(solution)/shard_map/exchange_attend/pallas_call | solution.py:592
  143.2 2.6 %settle.1 = (bf16[384,512]{1,0:T(8,128)(2,1)}, bf16[1024,512]{1,0:T(8,128)(2,1)}, f32[256,256]{1,0:T(8,128)}) custom-call(bf16[384,512]{1,0:T(8,128)(2,1)} %get-tuple-element.15.refs_0_, bf16[1024,512]{1,0:T(8,128)(2,1)} %get-tuple-element.16.refs_1_, f32[256,256]{1,0:T(8,128)} %get-tuple-element.17.refs_2_), custom_call_target="tpu_custom_call" | custom-call | tf_op jit(solution)/shard_map/settle/pallas_call | solution.py:217
  (7 shorter events, 0.1 us)
Async XLA Ops:
  1.8 13.9 %copy-start.1 = (s32[24]{0:T(128)}, s32[24]{0:T(128)S(1)}, u32[]{:S(2)}) copy-start(s32[24]{0:T(128)S(1)} %multiply_add_fusion.slot_ref) | copy-start | bytes 292
  15.0 0.8 copy-start
where the time goes:
time: 146 us
  Pallas kernels  139 us (95%)
  local copies, waits for them, and re-layouts  3.34 us (2%)
  other arithmetic  2.32 us (2%)
    pallas_call x1, Pallas kernels, main_call(): pl.pallas_call(functools.partial(main_kernel, st_count, (cap, per_block,...  127 us
    pallas_call x1, Pallas kernels, project_call(): pl.pallas_call(functools.partial(project_kernel, st_count), out_shape=(ja...  9.38 us

commit v1 on v0

--- a/solution.py
+++ b/solution.py
@@ -30,11 +30,14 @@
 
 
 def st_peer(me, step, st_count):
-    half = st_count // 2
-    side, place = me // half, lax.rem(me, half)
-    if step <= half:
-        return (1 - side) * half + lax.rem(place + step - 1, half)
-    return side * half + lax.rem(place + step - half, half)
+    if st_count & (st_count - 1):
+        return lax.rem(me + step, st_count)
+    flips = st_count - step
+    peer = me
+    for bit in range(st_count.bit_length() - 1):
+        if flips >> bit & 1:
+            peer = peer + (1 << bit) * (1 - 2 * lax.rem(me // (1 << bit), 2))
+    return peer
 
 
 def meet(st_count, with_st, with_tp=True):

time: 146 us -> 130 us (0.89)
  the two profiles are of different devices: /device:TPU:20 before, /device:TPU:0 now
where the time goes in v1:
time: 130 us; the launch traced here: 129 us
  Pallas kernels  123 us (95%)
  local copies, waits for them, and re-layouts  3.34 us (3%)
  other arithmetic  2.32 us (2%)
    pallas_call x1, Pallas kernels, main_call(): pl.pallas_call(functools.partial(main_kernel, st_count, (cap, per_block,...  108 us
    pallas_call x1, Pallas kernels, project_call(): pl.pallas_call(functools.partial(project_kernel, st_count), out_shape=(ja...  12.2 us
    pallas_call x1, Pallas kernels, settle_call(): pl.pallas_call(settle_kernel, out_shape=tuple((jax.ShapeDtypeStruct(x.sha...  2.63 us

profile of v1, /device:TPU:0, one launch (start us, length us, event | category | flops | bytes accessed | tf_op | source)
XLA Modules:
  0.0 129.4 jit_solution(10168756537154678783)
XLA Ops:
  0.6 0.8 copy.21
  1.4 0.1 reshape.171
  1.5 0.1 reshape.168
  1.6 0.2 convert_reduce_fusion.1
  1.8 0.0 copy-start.1
  1.8 0.6 select_reduce_fusion.request_ref
  2.4 0.6 pad.4.ids_ref
  3.0 12.2 %ids_project.1 = (s32[8,8,128]{2,1,0:T(8,128)}, bf16[1024,256]{1,0:T(8,128)(2,1)}, bf16[1024,512]{1,0:T(8,128)(2,1)}) custom-call(s32[8,128]{1,0:T(8,128)} %pad.4.ids_ref, bf16[1024,2048]{1,0:T(8,128)(2,1)} %bitcast.9, bf16[2048,256]{1,0:T(8,128)(2,1)} %kw_ref.3, bf16[2048,256]{1,0:T(8,128)(2,1)} %vw_ref.3), custom_call_target="tpu_custom_call" | custom-call | tf_op jit(solution)/shard_map/ids_project/pallas_call | solution.py:193
  15.2 0.8 slice.3
  15.9 0.8 broadcast_compare_fusion
  16.8 0.3 convert_reduce_fusion
  17.1 0.2 fusion.1
  17.2 0.1 copy.24
  17.3 0.1 reduce_or.12
  17.4 0.1 select_reduce_fusion.1
  17.6 0.1 copy.22
  17.7 0.1 reshape.170.local_ref
  17.7 0.0 copy-start
  17.8 0.1 iota_add_fusion
  17.8 0.7 add.59.code_ref
  18.5 0.0 copy-done.1
  18.5 0.0 copy-done
  18.5 108.2 %exchange_attend.1 = (bf16[384,512]{1,0:T(8,128)(2,1)}, bf16[1024,512]{1,0:T(8,128)(2,1)}, f32[256,256]{1,0:T(8,128)}) custom-call(s32[24]{0:T(128)} %copy-done, s32[24]{0:T(128)} %copy-done.1, s32[24]{0:T(128)} %select_reduce_fusion.request_ref, f32[2]{0:T(128)} %rate_ref.1, s32[1,1536]{1,0:T(1,128)} %add.59.code_ref, bf16[384,512]{1,0:T(8,128)(2,1)} %own_ref.1, ...), custom_call_target="tpu_custom_call" | custom-call | tf_op jit(solution)/shard_map/exchange_attend/pallas_call | solution.py:595
  126.7 2.6 %settle.1 = (bf16[384,512]{1,0:T(8,128)(2,1)}, bf16[1024,512]{1,0:T(8,128)(2,1)}, f32[256,256]{1,0:T(8,128)}) custom-call(bf16[384,512]{1,0:T(8,128)(2,1)} %get-tuple-element.15.refs_0_, bf16[1024,512]{1,0:T(8,128)(2,1)} %get-tuple-element.16.refs_1_, f32[256,256]{1,0:T(8,128)} %get-tuple-element.17.refs_2_), custom_call_target="tpu_custom_call" | custom-call | tf_op jit(solution)/shard_map/settle/pallas_call | solution.py:220
  (7 shorter events, 0.1 us)
Async XLA Ops:
  1.8 16.7 %copy-start.1 = (s32[24]{0:T(128)}, s32[24]{0:T(128)S(1)}, u32[]{:S(2)}) copy-start(s32[24]{0:T(128)S(1)} %multiply_add_fusion.slot_ref) | copy-start | bytes 292
  17.7 0.8 copy-start
